TPU v7x, 32 devices: a whole 2x2x4 slice. The times are simulated.
32 devices in a mesh: sp: 8 (over z, x), tp: 4 (over y, core).
Axes of the slice: x: 2, y: 2, z: 4, core: 2. Of those that a mesh axis runs over, the one named last changes fastest.
Arguments:
- query_narrow: bfloat16 [2048, 1024], P('sp', 'tp'), may hold values from -6 to 6
- key_narrow: bfloat16 [2048, 1024], P('sp', 'tp'), may hold values from -6 to 6
- value_narrow: bfloat16 [2048, 1024], P('sp', 'tp'), may hold values from -12 to 12
- query_broad: bfloat16 [2048, 1024], P('sp', 'tp'), may hold values from -6 to 6
- key_broad: bfloat16 [2048, 1024], P('sp', 'tp'), may hold values from -6 to 6
- value_broad: bfloat16 [2048, 1024], P('sp', 'tp'), may hold values from -12 to 12
- offset_narrow: bfloat16 [16, 2048], P('tp', 'sp'), as said below
- offset_broad: bfloat16 [8, 2048], P('tp', 'sp'), as said below
- residual: bfloat16 [2048, 2048], P(('sp', 'tp')), may hold values from -6 to 6
- out_narrow: bfloat16 [1024, 2048], P('tp'), may hold values from -0.25 to 0.25
- out_broad: bfloat16 [1024, 2048], P('tp'), may hold values from -0.25 to 0.25
- norm_gain: float32 [2048], replicated, may hold values from 0.1 to 1.9
- up_proj: bfloat16 [2048, 8192], P('sp', 'tp'), may hold values from -0.125 to 0.125
- down_proj: bfloat16 [8192, 2048], P('tp', 'sp'), may hold values from -0.0625 to 0.0625
Outputs:
- output: bfloat16 [2048, 2048], P(('sp', 'tp'))
Inputs may be any that keep to these rules, and one draw needn't show every extreme that they name: `offset_narrow`: additive score offsets of each head for each key position. `offset_broad`: additive score offsets of each head for each key position.
All inputs are finite; a program needn't handle non-finite values.
Results may differ from a plain program's by a relative error of at most 0.018.
Values may be sent and summed in bfloat16 or wider, within the bound.
A program may use at most 64 MiB of HBM per device.

v0:
```python
import math

import jax
import jax.numpy as jnp
from jax import lax
from jax.sharding import PartitionSpec as P

NARROW_SIZE = 64
BROAD_SIZE = 128


def stick_block(state, query, keys_block, values_block, offsets, query_pos, key_pos, head_size):
    keep_sum, running = state
    row_count = query.shape[0]
    total_heads = query.shape[1] // head_size
    key_count = keys_block.shape[0]
    q_heads = query.reshape(row_count, total_heads, head_size)
    k_heads = keys_block.reshape(key_count, total_heads, head_size)
    v_heads = values_block.reshape(key_count, total_heads, head_size)
    scores = jnp.einsum(
        "qhe,khe->hqk", q_heads, k_heads, preferred_element_type=jnp.float32
    ) * head_size ** (-0.5)
    scores = scores + offsets.astype(jnp.float32)[:, None, :]
    causal = (key_pos[None, :] < query_pos[:, None])[None]
    log_keep = jnp.where(causal, jax.nn.log_sigmoid(-scores), 0.0)
    keep_after = lax.cumsum(log_keep, axis=2, reverse=True) - log_keep
    weight = jnp.where(
        causal, jnp.exp(jax.nn.log_sigmoid(scores) + keep_after + keep_sum[:, :, None]), 0.0
    )
    weight = weight.astype(jnp.bfloat16)
    running = running + jnp.einsum(
        "hqk,khe->qhe", weight, v_heads, preferred_element_type=jnp.float32
    )
    return (keep_sum + jnp.sum(log_keep, axis=2), running)


def attend_block(states, pieces, query_pos, key_pos, queries):
    key_n, value_n, key_b, value_b, off_n, off_b = pieces
    state_narrow = stick_block(
        states[0], queries[0], key_n, value_n, off_n, query_pos, key_pos, NARROW_SIZE
    )
    state_broad = stick_block(
        states[1], queries[1], key_b, value_b, off_b, query_pos, key_pos, BROAD_SIZE
    )
    return (state_narrow, state_broad)


def local(
    query_narrow,
    key_narrow,
    value_narrow,
    query_broad,
    key_broad,
    value_broad,
    offset_narrow,
    offset_broad,
    residual,
    out_narrow,
    out_broad,
    norm_gain,
    up_proj,
    down_proj,
):
    tok_dev = query_narrow.shape[0]
    my_shard = lax.axis_index("sp")
    up_whole, down_whole = (
        lax.all_gather(up_proj, "sp", axis=0, tiled=True),
        lax.all_gather(down_proj, "sp", axis=1, tiled=True),
    )
    query_pos = my_shard * tok_dev + jnp.arange(tok_dev, dtype=jnp.int32)
    queries = (query_narrow, query_broad)

    def empty_state(total_heads, head_size):
        return (
            jnp.zeros((total_heads, tok_dev), jnp.float32),
            jnp.zeros((tok_dev, total_heads, head_size), jnp.float32),
        )

    states = (
        empty_state(offset_narrow.shape[0], NARROW_SIZE),
        empty_state(offset_broad.shape[0], BROAD_SIZE),
    )
    own_keys = (key_narrow, value_narrow, key_broad, value_broad, offset_narrow, offset_broad)
    whole_keys = (
        lax.all_gather(own_keys[0], "sp", axis=0, tiled=True),
        lax.all_gather(own_keys[1], "sp", axis=0, tiled=True),
        lax.all_gather(own_keys[2], "sp", axis=0, tiled=True),
        lax.all_gather(own_keys[3], "sp", axis=0, tiled=True),
        lax.all_gather(own_keys[4], "sp", axis=1, tiled=True),
        lax.all_gather(own_keys[5], "sp", axis=1, tiled=True),
    )
    key_span = math.gcd(tok_dev, 512)
    block_count = (my_shard + 1) * (tok_dev // key_span)

    def sweep(turn_index, current):
        first_row = (block_count - 1 - turn_index) * key_span
        row_pieces = tuple(
            (lax.dynamic_slice_in_dim(array, first_row, key_span, 0) for array in whole_keys[:4])
        )
        col_pieces = tuple(
            (lax.dynamic_slice_in_dim(array, first_row, key_span, 1) for array in whole_keys[4:])
        )
        key_pos = first_row + jnp.arange(key_span, dtype=jnp.int32)
        return attend_block(current, row_pieces + col_pieces, query_pos, key_pos, queries)

    states = lax.fori_loop(0, block_count, sweep, states)
    mixed_narrow = states[0][1].reshape(tok_dev, -1).astype(jnp.bfloat16)
    mixed_broad = states[1][1].reshape(tok_dev, -1).astype(jnp.bfloat16)
    attended = lax.psum_scatter(
        (
            jnp.dot(mixed_narrow, out_narrow, preferred_element_type=jnp.float32)
            + jnp.dot(mixed_broad, out_broad, preferred_element_type=jnp.float32)
        ).astype(jnp.bfloat16),
        "tp",
        scatter_dimension=0,
        tiled=True,
    ).astype(jnp.float32)
    updated = residual.astype(jnp.float32) + attended
    scale = lax.rsqrt(jnp.mean(updated * updated, axis=-1, keepdims=True) + 1e-06)
    normed = (updated * scale * norm_gain).astype(jnp.bfloat16)
    product = jnp.dot(
        lax.all_gather(normed, "tp", axis=0, tiled=True),
        up_whole,
        preferred_element_type=jnp.float32,
    )
    hidden = jnp.square(jax.nn.relu(product)).astype(jnp.bfloat16)
    channel = lax.psum_scatter(
        jnp.dot(hidden, down_whole, preferred_element_type=jnp.float32).astype(jnp.bfloat16),
        "tp",
        scatter_dimension=0,
        tiled=True,
    ).astype(jnp.float32)
    return (updated + channel).astype(jnp.bfloat16)


def solution(mesh):
    return jax.shard_map(
        local,
        mesh=mesh,
        in_specs=(
            P("sp", "tp"),
            P("sp", "tp"),
            P("sp", "tp"),
            P("sp", "tp"),
            P("sp", "tp"),
            P("sp", "tp"),
            P("tp", "sp"),
            P("tp", "sp"),
            P(("sp", "tp"), None),
            P("tp", None),
            P("tp", None),
            P(),
            P("sp", "tp"),
            P("tp", "sp"),
        ),
        out_specs=P(("sp", "tp"), None),
        check_vma=False,
    )
```

profile of v0, /device:TPU:19, one launch (start us, length us, event | category | flops | bytes accessed | tf_op | source)
XLA Modules:
  0.0 709.5 jit_solution(16716447176475630619)
XLA Ops:
  14.6 11.5 %all_gather.31 = bf16[2,2048]{1,0:T(2,128)(2,1)S(1)} all-gather(bf16[2,256]{1,0:T(2,128)(2,1)} %param.23), channel_id=1, replica_groups=mesh['sp'=8,'tp'=4] {'sp'}, dimensions={1}, use_global_device_ids=true | all-gather | bytes 9216 | tf_op jit(solution)/shard_map/all_gather | solution.py:90
  26.1 21.6 %all_gather.28 = bf16[4,2048]{1,0:T(4,128)(2,1)S(1)} all-gather(bf16[4,256]{1,0:T(4,128)(2,1)} %param.22), channel_id=1, replica_groups=mesh['sp'=8,'tp'=4] {'sp'}, dimensions={1}, use_global_device_ids=true | all-gather | bytes 18432 | tf_op jit(solution)/shard_map/all_gather | solution.py:89
  47.8 40.0 %all-gather.12.cloned.1.call-done = bf16[2048,256]{0,1:T(8,128)(2,1)} async-done(((bf16[256,256]{0,1:T(8,128)(2,1)}), bf16[2048,256]{0,1:T(8,128)(2,1)}) %all-gather.12.cloned.1.call-update) | async-done | bytes 1048592 | tf_op jit(solution)/shard_map/all_gather | solution.py:87
  87.7 40.5 %all-gather.14.cloned.1.call-done = bf16[2048,256]{0,1:T(8,128)(2,1)} async-done(((bf16[256,256]{0,1:T(8,128)(2,1)}), bf16[2048,256]{0,1:T(8,128)(2,1)}) %all-gather.14.cloned.1.call-update) | async-done | bytes 1048592 | tf_op jit(solution)/shard_map/all_gather | solution.py:88
  128.2 40.3 %all-gather.8.cloned.1.call-done = bf16[2048,256]{0,1:T(8,128)(2,1)} async-done(((bf16[256,256]{0,1:T(8,128)(2,1)}), bf16[2048,256]{0,1:T(8,128)(2,1)}) %all-gather.8.cloned.1.call-update) | async-done | bytes 1048592 | tf_op jit(solution)/shard_map/all_gather | solution.py:85
  170.0 146.0 %while.19 = (s32[]{:T(128)}, f32[4,256]{1,0:T(4,128)S(1)}, f32[256,4,64]{0,2,1:T(8,128)}, f32[2,256]{1,0:T(2,128)S(1)}, f32[256,2,128]{0,2,1:T(8,128)}, /*index=...) while((s32[]{:T(128)}, f32[4,256]{1,0:T(4,128)S(1)}, ...), condition=%wide.region_7.8_spmd.clone, body=%wide.region_0.7_spmd.clone.sunk | while | flops 197335552 | bytes 22752592 | solution.py:106
  172.6 4.6 fusion.88
  182.1 9.2 %fusion.83 = f32[4,256,2,128]{1,2,3,0:T(2,128)S(1)} fusion(f32[4,256,2,128]{1,3,2,0:T(8,128)S(1)} %bitcast.100), kind=kOutput, calls=%fused_computation.24.clone.1 | output fusion | flops 33292288 | bytes 2097152 | tf_op jit(solution)/shard_map/reduce-window.8
  196.9 4.6 fusion.88
  206.4 9.2 %fusion.83 = f32[4,256,2,128]{1,2,3,0:T(2,128)S(1)} fusion(f32[4,256,2,128]{1,3,2,0:T(8,128)S(1)} %bitcast.100), kind=kOutput, calls=%fused_computation.24.clone.1 | output fusion | flops 33292288 | bytes 2097152 | tf_op jit(solution)/shard_map/reduce-window.8
  221.3 4.6 fusion.88
  230.8 9.2 %fusion.83 = f32[4,256,2,128]{1,2,3,0:T(2,128)S(1)} fusion(f32[4,256,2,128]{1,3,2,0:T(8,128)S(1)} %bitcast.100), kind=kOutput, calls=%fused_computation.24.clone.1 | output fusion | flops 33292288 | bytes 2097152 | tf_op jit(solution)/shard_map/reduce-window.8
  245.6 4.6 fusion.88
  255.1 9.2 %fusion.83 = f32[4,256,2,128]{1,2,3,0:T(2,128)S(1)} fusion(f32[4,256,2,128]{1,3,2,0:T(8,128)S(1)} %bitcast.100), kind=kOutput, calls=%fused_computation.24.clone.1 | output fusion | flops 33292288 | bytes 2097152 | tf_op jit(solution)/shard_map/reduce-window.8
  269.9 4.6 fusion.88
  279.4 9.2 %fusion.83 = f32[4,256,2,128]{1,2,3,0:T(2,128)S(1)} fusion(f32[4,256,2,128]{1,3,2,0:T(8,128)S(1)} %bitcast.100), kind=kOutput, calls=%fused_computation.24.clone.1 | output fusion | flops 33292288 | bytes 2097152 | tf_op jit(solution)/shard_map/reduce-window.8
  294.2 4.6 fusion.88
  303.7 9.2 %fusion.83 = f32[4,256,2,128]{1,2,3,0:T(2,128)S(1)} fusion(f32[4,256,2,128]{1,3,2,0:T(8,128)S(1)} %bitcast.100), kind=kOutput, calls=%fused_computation.24.clone.1 | output fusion | flops 33292288 | bytes 2097152 | tf_op jit(solution)/shard_map/reduce-window.8
  320.0 74.8 %reduce-scatter.3.cloned.1.call-done = bf16[64,2048]{1,0:T(8,128)(2,1)} async-done(((bf16[256,2048]{1,0:T(8,128)(2,1)}), bf16[64,2048]{1,0:T(8,128)(2,1)}) %reduce-scatter.3.cloned.1.call-update) | async-done | bytes 262160 | tf_op jit(solution)/shard_map/reduce_scatter | solution.py:109
  399.4 15.8 %all-gather.16.cloned.1.call-done = bf16[256,2048]{1,0:T(8,128)(2,1)} async-done(((bf16[64,2048]{1,0:T(8,128)(2,1)}), bf16[256,2048]{1,0:T(8,128)(2,1)}) %all-gather.16.cloned.1.call-update) | async-done | bytes 1048592 | tf_op jit(solution)/shard_map/all_gather | solution.py:122
  415.2 123.7 %all-gather.18.cloned.1.call-done = bf16[2048,2048]{1,0:T(8,128)(2,1)} async-done(((bf16[256,2048]{1,0:T(8,128)(2,1)}), bf16[2048,2048]{1,0:T(8,128)(2,1)}) %all-gather.18.cloned.1.call-update) | async-done | bytes 8388624 | tf_op jit(solution)/shard_map/all_gather | solution.py:67
  538.9 125.2 %all-gather.20.cloned.1.call-done = bf16[2048,2048]{1,0:T(8,128)(2,1)} async-done(((bf16[2048,256]{1,0:T(8,128)(2,1)}), bf16[2048,2048]{1,0:T(8,128)(2,1)}) %all-gather.20.cloned.1.call-update) | async-done | bytes 8388624 | tf_op jit(solution)/shard_map/all_gather | solution.py:68
  664.1 11.5 %convolution_convert_fusion = bf16[256,2048]{1,0:T(8,128)(2,1)} fusion(bf16[2048,2048]{1,0:T(8,128)(2,1)} %all-gather.20.cloned.1.call-done, bf16[256,2048]{1,0:T(8,128)(2,1)} %all-gather.16.cloned.1.call-done, bf16[2048,2048]{1,0:T(8,128)(2,1)} %all-gather.18.cloned.1.call-done), kind=kOutput, calls=%fused_computation.60 | convolution fusion | flops 4297064448 | bytes 18874368 | tf_op jit(solution)/shard_map/dot_general | solution.py:128
  675.7 25.5 %reduce-scatter.5.cloned.1.call-done = bf16[64,2048]{1,0:T(8,128)(2,1)} async-done(((bf16[256,2048]{1,0:T(8,128)(2,1)}), bf16[64,2048]{1,0:T(8,128)(2,1)}) %reduce-scatter.5.cloned.1.call-update) | async-done | bytes 262160 | tf_op jit(solution)/shard_map/reduce_scatter | solution.py:127
  (214 shorter events, 81.9 us)
Async XLA Ops:
  6.5 311.5 %copy-start = (bf16[256,2048]{1,0:T(8,128)(2,1)S(1)}, bf16[256,2048]{1,0:T(8,128)(2,1)}, u32[]{:S(2)}) copy-start(bf16[256,2048]{1,0:T(8,128)(2,1)} %param.25) | copy-start | bytes 3145732
  6.5 41.2 %all-gather.10.cloned.1.call-start = ((), (), s32[]{:S(2)}) async-start(), calls=%async_computation.3 | async-start | bytes 1179648 | tf_op jit(solution)/shard_map/all_gather | solution.py:86
  8.3 79.4 %all-gather.12.cloned.1.call-start = ((), (), s32[]{:S(2)}) async-start(), calls=%async_computation.4 | async-start | bytes 1179648 | tf_op jit(solution)/shard_map/all_gather | solution.py:87
  10.1 118.2 %all-gather.14.cloned.1.call-start = ((), (), s32[]{:S(2)}) async-start(), calls=%async_computation.5 | async-start | bytes 1179648 | tf_op jit(solution)/shard_map/all_gather | solution.py:88
  11.8 156.8 %all-gather.8.cloned.1.call-start = ((), (), s32[]{:S(2)}) async-start(), calls=%async_computation.2 | async-start | bytes 1179648 | tf_op jit(solution)/shard_map/all_gather | solution.py:85
  13.5 381.3 %reduce-scatter.3.cloned.1.call-start = ((), (), s32[]{:S(2)}) async-start(), calls=%async_computation.6 | async-start | bytes 1310720 | tf_op jit(solution)/shard_map/reduce_scatter | solution.py:109
  191.7 1.6 copy-start.1
  193.6 0.7 copy-start.2
  216.1 1.6 copy-start.1
  240.4 1.6 copy-start.1
  242.3 0.7 copy-start.2
  264.7 1.6 copy-start.1
  266.6 0.7 copy-start.2
  289.1 1.6 copy-start.1
  290.9 0.7 copy-start.2
  313.4 1.6 copy-start.1
  316.0 2.5 copy-start.5
  318.5 76.4 %copy-start.3 = (bf16[64,2048]{1,0:T(8,128)(2,1)S(1)}, bf16[64,2048]{1,0:T(8,128)(2,1)}, u32[]{:S(2)}) copy-start(bf16[64,2048]{1,0:T(8,128)(2,1)} %param.24) | copy-start | bytes 786436
  318.5 77.5 %copy-start.6 = (f32[2048]{0:T(1024)S(1)}, f32[2048]{0:T(1024)}, u32[]{:S(2)}) copy-start(f32[2048]{0:T(1024)} %param.27) | copy-start | bytes 24580
  320.0 95.2 %all-gather.16.cloned.1.call-start = ((), (), s32[]{:S(2)}) async-start(), calls=%async_computation.7 | async-start | bytes 1310720 | tf_op jit(solution)/shard_map/all_gather | solution.py:122
  397.8 141.1 %all-gather.18.cloned.1.call-start = ((), (), s32[]{:S(2)}) async-start(), calls=%async_computation.8 | async-start | bytes 9437184 | tf_op jit(solution)/shard_map/all_gather | solution.py:67
  398.6 265.5 %all-gather.20.cloned.1.call-start = ((), (), s32[]{:S(2)}) async-start(), calls=%async_computation.9 | async-start | bytes 9437184 | tf_op jit(solution)/shard_map/all_gather | solution.py:68
  399.3 301.9 %copy-start.4 = (bf16[64,2048]{1,0:T(8,128)(2,1)S(1)}, bf16[64,2048]{1,0:T(8,128)(2,1)}, u32[]{:S(2)}) copy-start(bf16[64,2048]{1,0:T(8,128)(2,1)} %reduce-scatter.3.cloned.1.call-done) | copy-start | bytes 786436
  399.3 301.9 %reduce-scatter.5.cloned.1.call-start = ((), (), s32[]{:S(2)}) async-start(), calls=%async_computation.10 | async-start | bytes 1310720 | tf_op jit(solution)/shard_map/reduce_scatter | solution.py:127
  (2 other events, 1.4 us)
Sparse Core Ops, SparseCore 0:
  9.4 37.8 all-gather.9
  49.3 38.3 all-gather.11
  89.8 38.3 all-gather.13
  130.1 38.3 all-gather.7
  320.1 74.7 reduce-scatter.2
  397.9 17.2 all-gather.15
  417.3 121.5 all-gather.17
  541.0 123.1 all-gather.19
  675.8 25.3 reduce-scatter.4
where the time goes:
time: 712 us; the launch traced here: 709 us
  waiting for transfers between devices  487 us (68%)
  other arithmetic  108 us (15%)
  matrix products  40.2 us (6%)
  blocking collectives  33.2 us (5%)
  local copies, waits for them, and re-layouts  26.1 us (4%)
  between operations  13.3 us (2%)
    all_gather x1, waiting for transfers between devices, local(): lax.all_gather(down_proj, 'sp', axis=1, tiled=True)  125 us
    all_gather x1, waiting for transfers between devices, local(): lax.all_gather(up_proj, 'sp', axis=0, tiled=True)  124 us
    another operation x24, other arithmetic  83.2 us
    reduce_scatter x1, waiting for transfers between devices, local(): lax.psum_scatter((jnp.dot(mixed_narrow, out_narrow, preferred_element_typ...  74.8 us
    all_gather x1, waiting for transfers between devices, local(): lax.all_gather(own_keys[3], 'sp', axis=0, tiled=True)  40.5 us
    all_gather x1, waiting for transfers between devices, local(): lax.all_gather(own_keys[0], 'sp', axis=0, tiled=True)  40.3 us
    all_gather x1, waiting for transfers between devices, local(): lax.all_gather(own_keys[2], 'sp', axis=0, tiled=True)  40 us
    reduce_scatter x1, waiting for transfers between devices, local(): lax.psum_scatter(jnp.dot(hidden, down_whole, preferred_element_type=jnp.f...  25.5 us
  transfers between devices with their start and end apart: 9, of which 8 were waited for; matrix products, arithmetic and copies ran while one was open for 1% of the time, Pallas kernels for 0%

commit v1 on v0

v1 whole, which is shorter than its diff:
```python
import functools

import jax
import jax.numpy as jnp
from jax import lax
from jax.experimental import pallas as pl
from jax.experimental.pallas import tpu as pltpu
from jax.sharding import PartitionSpec as P

NARROW_SIZE = 64
BROAD_SIZE = 128
F32 = jnp.float32
BF16 = jnp.bfloat16


def ring_order(shards):
    across = 1 << ((shards.bit_length() - 1) // 2)
    along = shards // across
    order = [z * across for z in range(along)]
    for turn, z in enumerate(reversed(range(along))):
        row = list(range(1, across))
        if turn % 2:
            row.reverse()
        order += [z * across + x for x in row]
    return order


def lookup(table, index):
    found = jnp.int32(0)
    for place, value in enumerate(table):
        found = found + jnp.where(index == place, jnp.int32(value), jnp.int32(0))
    return found


def kernel(
    shards, peers, order,
    q_n, q_b, k_n, v_n, k_b, v_b, off_n, off_b, residual, out_n, out_b, gain, up, down,
    o_ref,
    kv_slots, off_slots, up_slots, down_slots, mixed, part, inbox, updated, normed_all,
    product, hidden, channel, send_sems, recv_sems, tp_send, tp_recv, load_sems,
):
    tok = q_n.shape[0]
    wide = product.shape[1]
    model = part.shape[2]
    rows = residual.shape[0]
    depth = up.shape[0]
    me = lax.axis_index("sp")
    me_tp = lax.axis_index("tp")
    inverse = [order.index(s) for s in range(shards)]
    pos = lookup(inverse, me)
    right = lookup(order, lax.rem(pos + 1, shards))
    left = lookup(order, lax.rem(pos + shards - 1, shards))

    half_up, half_down = wide // 2, wide // 2
    loads = []
    for way, (k, v, off) in enumerate(((k_n, v_n, off_n), (k_b, v_b, off_b))):
        loads += [
            (k, kv_slots.at[way, 0, pl.ds(0, tok)]),
            (v, kv_slots.at[way, 0, pl.ds(tok, tok)]),
            (off, off_slots.at[way, 0]),
        ]
    for way in range(2):
        loads += [
            (up.at[:, pl.ds(way * half_up, half_up)], up_slots.at[way, 0]),
            (down.at[pl.ds(way * half_down, half_down)], down_slots.at[way, 0]),
        ]
    loads = [
        pltpu.make_async_copy(src, dst, load_sems.at[i]) for i, (src, dst) in enumerate(loads)
    ]
    for load in loads:
        load.start()

    barrier = pltpu.get_barrier_semaphore()
    for shard in (left, right):
        pl.semaphore_signal(
            barrier, inc=1, device_id=(shard, me_tp), device_id_type=pl.DeviceIdType.MESH
        )
    for d in range(1, peers):
        pl.semaphore_signal(
            barrier, inc=1, device_id=(me, lax.rem(me_tp + d, peers)),
            device_id_type=pl.DeviceIdType.MESH,
        )
    pl.semaphore_wait(barrier, 1 + peers)

    def piece(stream, way, t):
        if stream == 0:
            return kv_slots.at[way, t]
        if stream == 1:
            return off_slots.at[way, t]
        if stream in (2, 3):
            size = depth // 2
            return up_slots.at[way, t, pl.ds((stream - 2) * size, size)]
        size = half_down // 2
        return down_slots.at[way, t, pl.ds((stream - 4) * size, size)]

    def hop(stream, way, t):
        return pltpu.make_async_remote_copy(
            src_ref=piece(stream, way, t),
            dst_ref=piece(stream, way, t + 1),
            send_sem=send_sems.at[way, stream, t],
            recv_sem=recv_sems.at[way, stream, t],
            device_id=((left if way else right), me_tp),
            device_id_type=pl.DeviceIdType.MESH,
        )

    def begin(streams, t):
        for stream in streams:
            for way in range(2):
                hop(stream, way, t).start()

    def relay(streams, t):
        for stream in streams:
            for way in range(2):
                hop(stream, way, t - 1).wait_recv()
                hop(stream, way, t).start()

    def arrive(streams):
        for stream in streams:
            for way in range(2):
                hop(stream, way, shards - 2).wait_recv()

    def each(first, last, body):
        def step(t, carry):
            body(t)
            return carry

        lax.fori_loop(first, last, step, 0)

    KEYS, UPS, DOWNS = (0, 1), (2, 3), (4, 5)
    for load in loads:
        load.wait()
    begin(KEYS, 0)
    each(1, shards - 1, functools.partial(relay, KEYS))
    begin(UPS, 0)
    arrive(KEYS)

    row_at = lax.broadcasted_iota(jnp.int32, (tok, tok), 0)
    col_at = lax.broadcasted_iota(jnp.int32, (tok, tok), 1)
    later = (row_at > col_at).astype(BF16)
    later2 = jnp.concatenate([later, later], axis=0)
    heads = []
    for way, (q, size) in enumerate(((q_n, NARROW_SIZE), (q_b, BROAD_SIZE))):
        for h in range(q.shape[1] // size):
            heads.append((way, h, size, q))

    def head_block(way, h, size, q, block, keep_sum, diagonal):
        there = lookup(inverse, block)
        slot = lax.rem((there - pos if way else pos - there) + shards, shards)
        cols = pl.ds(h * size, size)
        keys = kv_slots[way, slot, pl.ds(0, tok), cols]
        values = kv_slots[way, slot, pl.ds(tok, tok), cols]
        offset = off_slots[way, slot].astype(F32)[h : h + 1, :]
        scores = lax.dot_general(
            q[:, cols], keys, (((1,), (1,)), ((), ())), preferred_element_type=F32
        ) * (size ** -0.5) + offset
        keep = -(jnp.maximum(scores, 0.0) + jnp.log(1.0 + jnp.exp(-jnp.abs(scores))))
        breaks = scores + keep
        if diagonal:
            keep = jnp.where(col_at < row_at, keep, 0.0)
        high = keep.astype(BF16)
        low = (keep - high.astype(F32)).astype(BF16)
        after = jnp.dot(
            jnp.concatenate([high, low], axis=1), later2, preferred_element_type=F32
        )
        weight = jnp.exp(breaks + after + keep_sum)
        if diagonal:
            weight = jnp.where(col_at < row_at, weight, 0.0)
        added = jnp.dot(weight.astype(BF16), values, preferred_element_type=F32)
        return keep_sum + (after[:, :1] + keep[:, :1]), added

    for index, (way, h, size, q) in enumerate(heads):
        start = head_block(way, h, size, q, me, jnp.zeros((tok, 1), F32), True)

        def sweep(turn, state, way=way, h=h, size=size, q=q):
            keep_sum, running = state
            keep_sum, added = head_block(way, h, size, q, me - 1 - turn, keep_sum, False)
            return keep_sum, running + added

        _, running = lax.fori_loop(0, me, sweep, start)
        base = way * q_n.shape[1] + h * size
        mixed[:, pl.ds(base, size)] = running.astype(BF16)

    relay(UPS, 1)

    def tp_copy(src, dst, kind, d):
        return pltpu.make_async_remote_copy(
            src_ref=src, dst_ref=dst,
            send_sem=tp_send.at[kind, d - 1], recv_sem=tp_recv.at[kind, d - 1],
            device_id=(me, lax.rem(me_tp + d, peers)),
            device_id_type=pl.DeviceIdType.MESH,
        )

    def scatter(kind):
        copies = []
        for d in range(1, peers):
            peer = lax.rem(me_tp + d, peers)
            copies.append(
                tp_copy(
                    part.at[kind, pl.ds(pl.multiple_of(peer * rows, rows), rows)],
                    inbox.at[kind, d - 1], kind, d,
                )
            )
        for copy in copies:
            copy.start()
        return copies

    def summed(kind, copies):
        for copy in copies:
            copy.wait_recv()
        own = pl.multiple_of(me_tp * rows, rows)
        total = part[kind, pl.ds(own, rows), :].astype(F32)
        for d in range(1, peers):
            total = total + inbox[kind, d - 1].astype(F32)
        return total

    tile = min(512, model)
    n_cols = out_n.shape[0]

    def project(c):
        cols = pl.ds(pl.multiple_of(c * tile, tile), tile)
        part[0, :, cols] = (
            jnp.dot(mixed[:, :n_cols], out_n[:, cols], preferred_element_type=F32)
            + jnp.dot(mixed[:, n_cols:], out_b[:, cols], preferred_element_type=F32)
        ).astype(BF16)

    each(0, model // tile, project)
    first = scatter(0)
    relay(UPS, 2)
    updated[...] = residual[...].astype(F32) + summed(0, first)
    value = updated[...]
    scale = lax.rsqrt(jnp.mean(value * value, axis=-1, keepdims=True) + 1e-06)
    mine = pl.ds(pl.multiple_of(me_tp * rows, rows), rows)
    normed_all[mine, :] = (value * scale * gain[...]).astype(BF16)
    spread = [tp_copy(normed_all.at[mine], normed_all.at[mine], 2, d) for d in range(1, peers)]
    for copy in spread:
        copy.start()
    relay(UPS, 3)
    for copy in spread:
        copy.wait_recv()

    product[...] = jnp.zeros_like(product)
    channel[...] = jnp.zeros_like(channel)
    step_cols = min(512, half_up)

    def source(way, t):
        return lookup(order, lax.rem((pos + t if way else pos - t + shards), shards))

    def climb(t):
        for way in range(2):
            lhs_cols = pl.ds(pl.multiple_of(source(way, t) * depth, depth), depth)

            def one(c, way=way, lhs_cols=lhs_cols):
                at = pl.multiple_of(c * step_cols, step_cols)
                product[:, pl.ds(way * half_up + at, step_cols)] += jnp.dot(
                    normed_all[:, lhs_cols], up_slots[way, t, :, pl.ds(at, step_cols)],
                    preferred_element_type=F32,
                )

            each(0, half_up // step_cols, one)

    def descend(t):
        for way in range(2):
            cols = pl.ds(pl.multiple_of(source(way, t) * depth, depth), depth)
            channel[:, cols] += jnp.dot(
                hidden[:, pl.ds(way * half_down, half_down)], down_slots[way, t],
                preferred_element_type=F32,
            )

    each(0, 4, climb)

    def up_step(t):
        relay(UPS, t)
        climb(t)

    each(4, shards - 1, up_step)
    begin(DOWNS, 0)
    arrive(UPS)
    climb(shards - 1)

    def activate(c):
        cols = pl.ds(pl.multiple_of(c * step_cols, step_cols), step_cols)
        hidden[:, cols] = jnp.square(jnp.maximum(product[:, cols], 0.0)).astype(BF16)

    each(0, wide // step_cols, activate)
    descend(0)

    def down_step(t):
        relay(DOWNS, t)
        descend(t)

    each(1, shards - 1, down_step)
    arrive(DOWNS)
    descend(shards - 1)

    def settle(c):
        cols = pl.ds(pl.multiple_of(c * tile, tile), tile)
        part[1, :, cols] = channel[:, cols].astype(BF16)

    each(0, model // tile, settle)
    last = scatter(1)
    o_ref[...] = (updated[...] + summed(1, last)).astype(BF16)

    def drain(t):
        for stream in KEYS + UPS + DOWNS:
            for way in range(2):
                hop(stream, way, t).wait_send()

    each(0, shards - 1, drain)
    for copy in first + spread + last:
        copy.wait_send()


def local(
    shards, peers, order,
    query_narrow, key_narrow, value_narrow, query_broad, key_broad, value_broad,
    offset_narrow, offset_broad, residual, out_narrow, out_broad, norm_gain, up_proj, down_proj,
):
    tok, columns = query_narrow.shape
    rows, model = residual.shape
    depth, wide = up_proj.shape
    pad = 16

    def padded(offset):
        return jnp.pad(offset, ((0, pad - offset.shape[0]), (0, 0)))

    vmem = pl.BlockSpec(memory_space=pltpu.VMEM)
    anywhere = pl.BlockSpec(memory_space=pl.ANY)
    return pl.pallas_call(
        functools.partial(kernel, shards, peers, order),
        out_shape=jax.ShapeDtypeStruct((rows, model), BF16),
        in_specs=[vmem] * 2 + [anywhere] * 6 + [vmem] * 4 + [anywhere] * 2,
        out_specs=vmem,
        scratch_shapes=[
            pltpu.VMEM((2, shards, 2 * tok, columns), BF16),
            pltpu.VMEM((2, shards, pad, tok), BF16),
            pltpu.VMEM((2, shards, depth, wide // 2), BF16),
            pltpu.VMEM((2, shards, wide // 2, depth), BF16),
            pltpu.VMEM((tok, 2 * columns), BF16),
            pltpu.VMEM((2, tok, model), BF16),
            pltpu.VMEM((2, peers - 1, rows, model), BF16),
            pltpu.VMEM((rows, model), F32),
            pltpu.VMEM((tok, model), BF16),
            pltpu.VMEM((tok, wide), F32),
            pltpu.VMEM((tok, wide), BF16),
            pltpu.VMEM((tok, model), F32),
            pltpu.SemaphoreType.DMA((2, 6, shards)),
            pltpu.SemaphoreType.DMA((2, 6, shards)),
            pltpu.SemaphoreType.DMA((3, peers - 1)),
            pltpu.SemaphoreType.DMA((3, peers - 1)),
            pltpu.SemaphoreType.DMA((10,)),
        ],
        compiler_params=pltpu.CompilerParams(
            collective_id=0, has_side_effects=True, vmem_limit_bytes=60 << 20
        ),
    )(
        query_narrow, query_broad, key_narrow, value_narrow, key_broad, value_broad,
        padded(offset_narrow), padded(offset_broad), residual, out_narrow, out_broad,
        norm_gain.reshape(1, -1), up_proj, down_proj,
    )


def solution(mesh):
    shards, peers = mesh.shape["sp"], mesh.shape["tp"]
    return jax.shard_map(
        functools.partial(local, shards, peers, tuple(ring_order(shards))),
        mesh=mesh,
        in_specs=(
            P("sp", "tp"),
            P("sp", "tp"),
            P("sp", "tp"),
            P("sp", "tp"),
            P("sp", "tp"),
            P("sp", "tp"),
            P("tp", "sp"),
            P("tp", "sp"),
            P(("sp", "tp"), None),
            P("tp", None),
            P("tp", None),
            P(),
            P("sp", "tp"),
            P("tp", "sp"),
        ),
        out_specs=P(("sp", "tp"), None),
        check_vma=False,
    )
```

time: 712 us -> 245 us (0.34)
  waiting for transfers between devices: 487 us -> 0 us
  Pallas kernels: 0 us -> 241 us
  other arithmetic: 108 us -> 0 us
  matrix products: 40.2 us -> 0 us
  blocking collectives: 33.2 us -> 0 us
  local copies, waits for them, and re-layouts: 26.1 us -> 3.57 us
  between operations: 13.3 us -> 0.01 us
    all_gather x7 -> x0, waiting for transfers between devices: 386 us -> none  [the longest x1 125 us: local(): lax.all_gather(down_proj, 'sp', axis=1, tiled=True)]
    pallas_call x0 -> x1, Pallas kernels: none -> 241 us  [local(): pl.pallas_call(functools.partial(kernel, shards, peers, order), out_shape...]
    reduce_scatter x2 -> x0, waiting for transfers between devices: 100 us -> none  [the longest x1 74.8 us: local(): lax.psum_scatter((jnp.dot(mixed_narrow, out_narrow, preferred_element_typ...]
    another operation x36 -> x0, other arithmetic: 86.6 us -> none
    dot_general x27 -> x0, matrix products: 40.2 us -> none  [the longest x12 14.4 us: stick_block(): jnp.einsum('qhe,khe->hqk', q_heads, k_heads, preferred_element_type=jnp.f...]
    all_gather x2 -> x0, blocking collectives: 33.2 us -> none  [the longest x1 21.6 us: local(): lax.all_gather(own_keys[4], 'sp', axis=1, tiled=True)]
    convert_element_type x28 -> x0, other arithmetic: 19.6 us -> none  [the longest x12 13.9 us: stick_block(): weight = weight.astype(jnp.bfloat16)]
    dynamic_slice x12 -> x0, local copies, waits for them, and re-layouts: 11.8 us -> none  [sweep(): lax.dynamic_slice_in_dim(array, first_row, key_span, 0)]
  transfers between devices with their start and end apart: 9 -> 0, of which waited for: 8 -> 0; matrix products, arithmetic and copies ran while one was open for 1% -> 0% of each run, Pallas kernels for 0% -> 0%
where the time goes in v1:
time: 245 us
  Pallas kernels  241 us (98%)
  local copies, waits for them, and re-layouts  3.57 us (1%)
    pallas_call x1, Pallas kernels, local(): pl.pallas_call(functools.partial(kernel, shards, peers, order), out_shape...  241 us

profile of v1, /device:TPU:19, one launch (start us, length us, event | category | flops | bytes accessed | tf_op | source)
XLA Modules:
  0.0 244.9 jit_solution(838431396612146602)
XLA Ops:
  0.0 0.0 copy-start
  0.0 1.3 pad.8.off_n
  1.3 0.0 copy-done
  1.3 0.6 pad.9.off_b
  1.9 241.3 %shard_map.136 = bf16[64,2048]{1,0:T(8,128)(2,1)} custom-call(bf16[256,256]{1,0:T(8,128)(2,1)} %q_n.1, bf16[256,256]{1,0:T(8,128)(2,1)} %q_b.1, bf16[256,256]{1,0:T(8,128)(2,1)} %k_n.1, bf16[256,256]{1,0:T(8,128)(2,1)} %v_n.1, bf16[256,256]{1,0:T(8,128)(2,1)} %k_b.1, bf16[256,256]{1,0:T(8,128)(2,1)} %v_b.1, bf16[16,256]{1,0:T(8,128)(2,1)} %pad.8.off_n, ...), custom_call_target="tpu_custom_call" | custom-call | tf_op jit(solution)/shard_map/pallas_call | solution.py:328
  243.2 1.7 copy.16
Async XLA Ops:
  0.0 1.3 copy-start

commit v2 on v1

--- a/solution.py
+++ b/solution.py
@@ -84,14 +84,14 @@
 
     def piece(stream, way, t):
         if stream == 0:
-            return kv_slots.at[way, t]
-        if stream == 1:
             return off_slots.at[way, t]
-        if stream in (2, 3):
+        if stream in (1, 2):
+            return kv_slots.at[way, t, pl.ds((stream - 1) * tok, tok)]
+        if stream in (3, 4):
             size = depth // 2
-            return up_slots.at[way, t, pl.ds((stream - 2) * size, size)]
+            return up_slots.at[way, t, pl.ds((stream - 3) * size, size)]
         size = half_down // 2
-        return down_slots.at[way, t, pl.ds((stream - 4) * size, size)]
+        return down_slots.at[way, t, pl.ds((stream - 5) * size, size)]
 
     def hop(stream, way, t):
         return pltpu.make_async_remote_copy(
@@ -126,7 +126,7 @@
 
         lax.fori_loop(first, last, step, 0)
 
-    KEYS, UPS, DOWNS = (0, 1), (2, 3), (4, 5)
+    KEYS, UPS, DOWNS = (0, 1, 2), (3, 4), (5, 6)
     for load in loads:
         load.wait()
     begin(KEYS, 0)
@@ -168,6 +168,7 @@
         added = jnp.dot(weight.astype(BF16), values, preferred_element_type=F32)
         return keep_sum + (after[:, :1] + keep[:, :1]), added
 
+    turn_up = 1
     for index, (way, h, size, q) in enumerate(heads):
         start = head_block(way, h, size, q, me, jnp.zeros((tok, 1), F32), True)
 
@@ -179,8 +180,9 @@
         _, running = lax.fori_loop(0, me, sweep, start)
         base = way * q_n.shape[1] + h * size
         mixed[:, pl.ds(base, size)] = running.astype(BF16)
-
-    relay(UPS, 1)
+        if index % 2:
+            relay(UPS, turn_up)
+            turn_up += 1
 
     def tp_copy(src, dst, kind, d):
         return pltpu.make_async_remote_copy(
@@ -225,7 +227,7 @@
 
     each(0, model // tile, project)
     first = scatter(0)
-    relay(UPS, 2)
+    relay(UPS, turn_up)
     updated[...] = residual[...].astype(F32) + summed(0, first)
     value = updated[...]
     scale = lax.rsqrt(jnp.mean(value * value, axis=-1, keepdims=True) + 1e-06)
@@ -234,7 +236,7 @@
     spread = [tp_copy(normed_all.at[mine], normed_all.at[mine], 2, d) for d in range(1, peers)]
     for copy in spread:
         copy.start()
-    relay(UPS, 3)
+    relay(UPS, turn_up + 1)
     for copy in spread:
         copy.wait_recv()
 
@@ -266,13 +268,13 @@
                 preferred_element_type=F32,
             )
 
-    each(0, 4, climb)
+    each(0, turn_up + 2, climb)
 
     def up_step(t):
         relay(UPS, t)
         climb(t)
 
-    each(4, shards - 1, up_step)
+    each(turn_up + 2, shards - 1, up_step)
     begin(DOWNS, 0)
     arrive(UPS)
     climb(shards - 1)
@@ -343,8 +345,8 @@
             pltpu.VMEM((tok, wide), F32),
             pltpu.VMEM((tok, wide), BF16),
             pltpu.VMEM((tok, model), F32),
-            pltpu.SemaphoreType.DMA((2, 6, shards)),
-            pltpu.SemaphoreType.DMA((2, 6, shards)),
+            pltpu.SemaphoreType.DMA((2, 7, shards)),
+            pltpu.SemaphoreType.DMA((2, 7, shards)),
             pltpu.SemaphoreType.DMA((3, peers - 1)),
             pltpu.SemaphoreType.DMA((3, peers - 1)),
             pltpu.SemaphoreType.DMA((10,)),

time: 245 us -> 226 us (0.922)
  Pallas kernels: 241 us -> 221 us
    pallas_call x1, Pallas kernels: 241 us -> 221 us  [local(): pl.pallas_call(functools.partial(kernel, shards, peers, order), out_shape...]
where the time goes in v2:
time: 226 us; the launch traced here: 224 us
  Pallas kernels  221 us (98%)
  local copies, waits for them, and re-layouts  3.57 us (2%)
    pallas_call x1, Pallas kernels, local(): pl.pallas_call(functools.partial(kernel, shards, peers, order), out_shape...  221 us

profile of v2, /device:TPU:19, one launch (start us, length us, event | category | flops | bytes accessed | tf_op | source)
XLA Modules:
  0.0 224.4 jit_solution(14054761730773502709)
XLA Ops:
  0.0 0.0 copy-start
  0.0 1.3 pad.8.off_n
  1.3 0.0 copy-done
  1.3 0.6 pad.9.off_b
  1.9 220.8 %shard_map.136 = bf16[64,2048]{1,0:T(8,128)(2,1)} custom-call(bf16[256,256]{1,0:T(8,128)(2,1)} %q_n.1, bf16[256,256]{1,0:T(8,128)(2,1)} %q_b.1, bf16[256,256]{1,0:T(8,128)(2,1)} %k_n.1, bf16[256,256]{1,0:T(8,128)(2,1)} %v_n.1, bf16[256,256]{1,0:T(8,128)(2,1)} %k_b.1, bf16[256,256]{1,0:T(8,128)(2,1)} %v_b.1, bf16[16,256]{1,0:T(8,128)(2,1)} %pad.8.off_n, ...), custom_call_target="tpu_custom_call" | custom-call | tf_op jit(solution)/shard_map/pallas_call | solution.py:330
  222.8 1.7 copy.16
Async XLA Ops:
  0.0 1.3 copy-start
